TPU v7x, 32 devices: a whole 2x2x4 slice. The times are simulated.
32 devices in a mesh: ep: 16 (over z, y, x), tp: 2 (over core).
Axes of the slice: x: 2, y: 2, z: 4, core: 2. Of those that a mesh axis runs over, the one named last changes fastest.
Arguments:
- tokens: bfloat16 [256, 2048], P('ep'), may hold values from -6 to 6
- state: float32 [256, 8, 128, 128], P('ep', 'tp'), may hold values from -6 to 6
- mix_gain: float32 [2048], replicated, may hold values from 0.1 to 1.9
- moe_gain: float32 [2048], replicated, may hold values from 0.1 to 1.9
- head_gain: float32 [128], replicated, may hold values from 0.1 to 1.9
- w_forget: bfloat16 [2048, 1024], P(None, 'tp'), may hold values from -0.125 to 0.125
- w_query: bfloat16 [2048, 1024], P(None, 'tp'), may hold values from -0.125 to 0.125
- w_input: bfloat16 [2048, 1024], P(None, 'tp'), may hold values from -0.125 to 0.125
- w_outgate: bfloat16 [2048, 1024], P(None, 'tp'), may hold values from -0.125 to 0.125
- lower_bound: float32 [1024], P('tp'), may hold values from 0 to 0.9
- w_mix_out: bfloat16 [1024, 2048], P('tp'), may hold values from -0.1875 to 0.1875
- routes: int32 [256, 6], P('ep'), may hold values from 0 to 15, all different within a row; in each aligned block of 16 rows (0 to 15, 16 to 31, ...) at most 16 rows name the same one
- route_scores: float32 [256, 6], P('ep'), may hold values from 0.05 to 1
- expert_gate: bfloat16 [16, 2048, 512], P('ep', None, 'tp'), may hold values from -0.125 to 0.125
- expert_up: bfloat16 [16, 2048, 512], P('ep', None, 'tp'), may hold values from -0.125 to 0.125
- expert_down: bfloat16 [16, 512, 2048], P('ep', 'tp'), may hold values from -0.25 to 0.25
- shared_gate: bfloat16 [2048, 512], P(None, 'tp'), may hold values from -0.125 to 0.125
- shared_up: bfloat16 [2048, 512], P(None, 'tp'), may hold values from -0.125 to 0.125
- shared_down: bfloat16 [512, 2048], P('tp'), may hold values from -0.25 to 0.25
Outputs:
- layer_out: bfloat16 [256, 2048], P('ep', 'tp')
- new_state: float32 [256, 8, 128, 128], P('ep', 'tp')
Inputs may be any that keep to these rules, and one draw needn't show every extreme that they name: `routes`: each token names 6 different experts. Among the tokens of one index of ep no expert is named by more than 16 tokens, and in every draw some expert is named by exactly 16 tokens of some index of ep.
All inputs are finite; a program needn't handle non-finite values.
Results may differ from a plain program's by a relative error of at most 0.017.
Values may be sent and summed in bfloat16 or wider, within the bound.
A program may use at most 128 MiB of HBM per device.

v0:
```python
import jax
import jax.numpy as jnp
from jax import lax
from jax.sharding import PartitionSpec as P

epsilon = 1e-06
routed_scale = 2.5


def rms_scale(values, gain):
    return values * lax.rsqrt(jnp.mean(values * values, axis=-1, keepdims=True) + epsilon) * gain


def local(
    tokens,
    state,
    mix_gain,
    moe_gain,
    head_gain,
    w_forget,
    w_query,
    w_input,
    w_outgate,
    lower_bound,
    w_mix_out,
    routes,
    route_scores,
    expert_gate,
    expert_up,
    expert_down,
    shared_gate,
    shared_up,
    shared_down,
):
    seqs_here = tokens.shape[0]
    heads_here = state.shape[1]
    key_width = state.shape[2]
    value_width = state.shape[3]
    tokens_wide = tokens.astype(jnp.float32)
    normed = rms_scale(tokens_wide, mix_gain).astype(jnp.bfloat16)
    forget_pre = jnp.dot(normed, w_forget, preferred_element_type=jnp.float32).reshape(
        seqs_here, heads_here, key_width
    )
    query = jax.nn.silu(jnp.dot(normed, w_query, preferred_element_type=jnp.float32)).reshape(
        seqs_here, heads_here, key_width
    )
    input_val = jnp.dot(normed, w_input, preferred_element_type=jnp.float32).reshape(
        seqs_here, heads_here, value_width
    )
    gate_pre = jnp.dot(normed, w_outgate, preferred_element_type=jnp.float32).reshape(
        seqs_here, heads_here, value_width
    )
    bound_rows = lower_bound.reshape(heads_here, key_width)
    forget = bound_rows + (1.0 - bound_rows) * jax.nn.sigmoid(forget_pre)
    key_gate = (1.0 - bound_rows) * jax.nn.sigmoid(-forget_pre)
    new_state = forget[..., None] * state + key_gate[..., None] * input_val[:, :, None, :]
    readout = jnp.einsum("shkv,shk->shv", new_state, query, precision=lax.Precision.HIGHEST)
    gated_out = (rms_scale(readout, head_gain) * jax.nn.silu(gate_pre)).astype(jnp.bfloat16)
    gated_out = gated_out.reshape(seqs_here, heads_here * value_width)
    partial_value = jnp.dot(gated_out, w_mix_out, preferred_element_type=jnp.float32)
    mixer_out = lax.psum(partial_value.astype(jnp.bfloat16), "tp")
    residual = tokens_wide + mixer_out.astype(jnp.float32)
    moe_rows = rms_scale(residual, moe_gain).astype(jnp.bfloat16)
    full_width = moe_rows.shape[1]
    half_width = full_width // 2
    tp_index = lax.axis_index("tp")
    shared_hidden = (
        jax.nn.silu(jnp.dot(moe_rows, shared_gate, preferred_element_type=jnp.float32))
        * jnp.dot(moe_rows, shared_up, preferred_element_type=jnp.float32)
    ).astype(jnp.bfloat16)
    shared_part = jnp.dot(shared_hidden, shared_down, preferred_element_type=jnp.float32)
    shared_out = lax.psum_scatter(
        shared_part.astype(jnp.bfloat16), "tp", scatter_dimension=1, tiled=True
    )
    top_count = routes.shape[1]
    experts_all = expert_gate.shape[0] * lax.axis_size("ep")
    capacity = max(2, min(seqs_here, seqs_here * top_count * 3 // experts_all))
    flat_routes = routes.reshape(-1)
    onehot = (flat_routes[:, None] == jnp.arange(experts_all, dtype=jnp.int32)[None, :]).astype(
        jnp.int32
    )
    earlier = jnp.cumsum(onehot, axis=0) - onehot
    slot_rank = jnp.sum(earlier * onehot, axis=1)
    slot_index = flat_routes * capacity + slot_rank
    placing = (
        slot_index[None, :] == jnp.arange(experts_all * capacity, dtype=jnp.int32)[:, None]
    ).astype(jnp.int32)
    placing = (
        placing.reshape(experts_all * capacity, seqs_here, top_count)
        .sum(axis=2)
        .astype(jnp.bfloat16)
    )
    own_columns = lax.dynamic_slice_in_dim(moe_rows, tp_index * half_width, half_width, 1)
    outgoing = jnp.dot(placing, own_columns, preferred_element_type=jnp.float32).astype(
        jnp.bfloat16
    )
    outgoing = outgoing.reshape(experts_all, capacity, half_width)
    arrived_half = lax.all_to_all(outgoing, "ep", split_axis=0, concat_axis=1, tiled=True)
    arrived = lax.all_gather(arrived_half, "tp", axis=2, tiled=True)
    gate_act = jnp.einsum("esd,edf->esf", arrived, expert_gate, preferred_element_type=jnp.float32)
    up_act = jnp.einsum("esd,edf->esf", arrived, expert_up, preferred_element_type=jnp.float32)
    expert_hidden = (jax.nn.silu(gate_act) * up_act).astype(jnp.bfloat16)
    expert_part = jnp.einsum(
        "esf,efd->esd", expert_hidden, expert_down, preferred_element_type=jnp.float32
    )
    expert_half = lax.psum_scatter(
        expert_part.astype(jnp.bfloat16), "tp", scatter_dimension=2, tiled=True
    )
    returned = lax.all_to_all(expert_half, "ep", split_axis=1, concat_axis=0, tiled=True)
    pair_out = returned.reshape(experts_all * capacity, half_width)[slot_index].astype(jnp.float32)
    weights = route_scores / jnp.sum(route_scores, axis=-1, keepdims=True) * routed_scale
    routed = jnp.sum(
        pair_out.reshape(seqs_here, top_count, half_width) * weights[:, :, None], axis=1
    )
    residual_half = lax.dynamic_slice_in_dim(residual, tp_index * half_width, half_width, 1)
    layer_out = (residual_half + routed + shared_out.astype(jnp.float32)).astype(jnp.bfloat16)
    return (layer_out, new_state)


def solution(mesh):
    return jax.shard_map(
        local,
        mesh=mesh,
        in_specs=(
            P("ep", None),
            P("ep", "tp", None, None),
            P(),
            P(),
            P(),
            P(None, "tp"),
            P(None, "tp"),
            P(None, "tp"),
            P(None, "tp"),
            P("tp"),
            P("tp", None),
            P("ep", None),
            P("ep", None),
            P("ep", None, "tp"),
            P("ep", None, "tp"),
            P("ep", "tp", None),
            P(None, "tp"),
            P(None, "tp"),
            P("tp", None),
        ),
        out_specs=(P("ep", "tp"), P("ep", "tp", None, None)),
        check_vma=False,
    )
```

profile of v0, /device:TPU:0, one launch (start us, length us, event | category | flops | bytes accessed | tf_op | source)
XLA Modules:
  0.0 138.7 jit_solution(9879463072840509546)
XLA Ops:
  7.2 1.1 fusion.18
  8.4 2.1 %fusion.40 = f32[16,512]{1,0:T(8,128)S(1)} fusion(bf16[2048,512]{1,0:T(8,128)(2,1)} %param.27, bf16[16,2048]{1,0:T(8,128)(2,1)} %param.19, f32[2048]{0:T(1024)} %param.21, f32[16]{0:T(128)S(1)} %add_rsqrt_fusion.2), kind=kOutput, calls=%fused_computation.72 | convolution fusion | flops 33685504 | bytes 2203712 | tf_op jit(solution)/shard_map/dot_general | solution.py:50
  10.5 2.0 %fusion.44 = f32[16,512]{1,0:T(8,128)S(1)} fusion(bf16[2048,512]{1,0:T(8,128)(2,1)} %param.26, bf16[16,2048]{1,0:T(8,128)(2,1)S(1)} %copy-done.3, f32[2048]{0:T(1024)S(1)} %copy-done.5, f32[16]{0:T(128)S(1)} %add_rsqrt_fusion.2), kind=kOutput, calls=%fused_computation.74 | convolution fusion | flops 33685504 | bytes 2203712 | tf_op jit(solution)/shard_map/dot_general | solution.py:47
  12.5 2.0 %add_divide_fusion.1 = (f32[16,512]{1,0:T(8,128)S(1)}, f32[16,512]{1,0:T(8,128)S(1)}) fusion(bf16[2048,512]{1,0:T(8,128)(2,1)} %param.24, bf16[16,2048]{1,0:T(8,128)(2,1)S(1)} %copy-done.3, f32[2048]{0:T(1024)S(1)} %copy-done.5, f32[16]{0:T(128)S(1)} %add_rsqrt_fusion.2), kind=kOutput, calls=%fused_computation.46 | convolution fusion | flops 33726464 | bytes 2236480 | tf_op jit(solution)/shard_map/dot_general | solution.py:41
  14.6 2.0 %divide_multiply_fusion.1 = f32[16,512]{1,0:T(8,128)S(1)} fusion(bf16[2048,512]{1,0:T(8,128)(2,1)} %param.25, bf16[16,2048]{1,0:T(8,128)(2,1)S(1)} %copy-done.3, f32[2048]{0:T(1024)S(1)} %copy-done.5, f32[16]{0:T(128)S(1)} %add_rsqrt_fusion.2), kind=kOutput, calls=%fused_computation.43 | convolution fusion | flops 33718272 | bytes 2203712 | tf_op jit(solution)/shard_map/dot_general | solution.py:44
  16.7 4.4 %multiply_add_fusion = f32[16,4,128,128]{3,2,1,0:T(8,128)S(1)} fusion(f32[16,4,128,128]{3,2,1,0:T(8,128)} %param.20, f32[16,4,128]{2,1,0:T(4,128)S(1)} %mul.181, f32[16,4,128]{2,1,0:T(4,128)S(1)} %bitcast.70, f32[16,4,128]{2,1,0:T(4,128)S(1)} %bitcast.69), kind=kLoop, calls=%fused_computation.1 | loop fusion | flops 3145728 | bytes 8486912 | tf_op jit(solution)/shard_map/add | solution.py:56
  21.2 3.7 %fusion.50 = f32[16,4,1,128]{3,2,1,0:T(1,128)S(1)} fusion(f32[16,4,128,128]{3,2,1,0:T(8,128)S(1)} %multiply_add_fusion, f32[16,4,128,1]{2,3,1,0:T(1,128)S(1)} %bitcast.71), kind=kOutput, calls=%fused_computation.77 | convolution fusion | flops 12582912 | bytes 4259840 | tf_op jit(solution)/shard_map/shkv,shk->shv/dot_general | solution.py:57
  27.0 19.7 %all-reduce.2.cloned.1.call-done = bf16[16,2048]{1,0:T(8,128)(2,1)} async-done(((bf16[16,2048]{1,0:T(8,128)(2,1)}), bf16[16,2048]{1,0:T(8,128)(2,1)}) %all-reduce.2.cloned.1.call-update) | async-done | bytes 65552 | tf_op jit(solution)/shard_map/psum | solution.py:61
  46.8 1.6 %convert_add_fusion = (f32[16,2048]{1,0:T(8,128)}, f32[16]{0:T(128)S(1)}) fusion(bf16[16,2048]{1,0:T(8,128)(2,1)S(1)} %copy-done.3, bf16[16,2048]{1,0:T(8,128)(2,1)} %all-reduce.2.cloned.1.call-done), kind=kLoop, calls=%fused_computation.24 | loop fusion | flops 163824 | bytes 262208 | tf_op jit(solution)/shard_map/add | solution.py:62
  49.6 22.2 %all_to_all.21 = bf16[16,16,1024]{2,1,0:T(8,128)(2,1)} all-to-all(bf16[16,16,1024]{2,1,0:T(8,128)(2,1)S(1)} %bitcast.66), channel_id=1, replica_groups=mesh['ep'=16,'tp'=2] {'ep'}, dimensions={0} | all-to-all | bytes 1048576 | tf_op jit(solution)/shard_map/all_to_all | solution.py:98
  72.1 7.3 %all-gather.2.cloned.1.call-done = bf16[1,256,2048]{2,1,0:T(8,128)(2,1)} async-done(((bf16[1,256,1024]{2,1,0:T(8,128)(2,1)}), bf16[1,256,2048]{2,1,0:T(8,128)(2,1)}) %all-gather.2.cloned.1.call-update) | async-done | bytes 1048592 | tf_op jit(solution)/shard_map/all_gather | solution.py:99
  79.4 2.1 %fusion.5 = f32[256,256]{1,0:T(8,128)S(1)} fusion(bf16[1,2048,256]{2,1,0:T(8,128)(2,1)} %param.32, bf16[1,256,2048]{2,1,0:T(8,128)(2,1)} %all-gather.2.cloned.1.call-done), kind=kOutput, calls=%fused_computation.13 | convolution fusion | flops 268435456 | bytes 2359296 | tf_op jit(solution)/shard_map/esd,edf->esf/dot_general | solution.py:100
  81.5 3.8 %fusion = bf16[1,256,2048]{2,1,0:T(8,128)(2,1)} fusion(bf16[1,256,2048]{2,1,0:T(8,128)(2,1)} %param.34, bf16[1,2048,256]{2,1,0:T(8,128)(2,1)} %param.33, bf16[1,256,2048]{2,1,0:T(8,128)(2,1)S(1)} %copy-done.2, f32[256,256]{1,0:T(8,128)S(1)} %fusion.5), kind=kOutput, calls=%fused_computation.3 | convolution fusion | flops 537788416 | bytes 4456448 | tf_op jit(solution)/shard_map/esf,efd->esd/dot_general | solution.py:103
  85.5 9.6 %reduce-scatter.3.cloned.1.call-done = bf16[1,256,1024]{2,1,0:T(8,128)(2,1)} async-done(((bf16[1,256,2048]{2,1,0:T(8,128)(2,1)}), bf16[1,256,1024]{2,1,0:T(8,128)(2,1)}) %reduce-scatter.3.cloned.1.call-update) | async-done | bytes 524304 | tf_op jit(solution)/shard_map/reduce_scatter | solution.py:106
  95.1 1.9 %copy.51 = bf16[1,256,1024]{2,0,1:T(2,128)(2,1)S(1)} copy(bf16[1,256,1024]{2,1,0:T(8,128)(2,1)} %reduce-scatter.3.cloned.1.call-done) | data formatting | bytes 1048576 | tf_op jit(solution)/shard_map/reduce_scatter | solution.py:106
  97.4 4.5 %reduce = bf16[256,1024]{1,0:T(8,128)(2,1)} reduce(bf16[256,1,1024]{2,1,0:T(2,128)(2,1)S(1)} %bitcast.64, bf16[]{:T(256)} %broadcast.158), dimensions={1}, to_apply=%bitcast.55.reduce_sub_computation | reduce | bytes 1048578
  101.9 2.2 %reshape.191 = bf16[16,2,8192]{2,1,0:T(2,128)(2,1)} reshape(bf16[256,1024]{1,0:T(8,128)(2,1)} %reduce) | data formatting | bytes 1048576
  104.1 6.8 %all-to-all-start.1 = ((bf16[16,2,8192]{2,1,0:T(2,128)(2,1)}), bf16[16,2,8192]{2,1,0:T(2,128)(2,1)S(1)}, u32[]{:S(2)}, u32[]{:S(2)}) async-start(bf16[16,2,8192]{2,1,0:T(2,128)(2,1)} %reshape.191), calls=%async_computation.2 | async-start | bytes 1048576 | tf_op jit(solution)/shard_map/all_to_all | solution.py:109
  111.1 1.5 %fusion.51 = f32[16,256]{1,0:T(8,128)S(1)} fusion(bf16[16,2048]{1,0:T(8,128)(2,1)S(1)} %multiply_convert_fusion, bf16[2048,256]{1,0:T(8,128)(2,1)} %param.35), kind=kOutput, calls=%fused_computation.78 | convolution fusion | flops 16777216 | bytes 1130496 | tf_op jit(solution)/shard_map/dot_general | solution.py:68
  112.6 2.9 %convolution_convert_fusion.1 = bf16[16,2048]{1,0:T(8,128)(2,1)} fusion(bf16[256,2048]{1,0:T(8,128)(2,1)} %param.37, bf16[16,2048]{1,0:T(8,128)(2,1)S(1)} %multiply_convert_fusion, bf16[2048,256]{1,0:T(8,128)(2,1)} %param.36, f32[16,256]{1,0:T(8,128)S(1)} %fusion.51), kind=kOutput, calls=%fused_computation.4 | convolution fusion | flops 33611776 | bytes 2244608 | tf_op jit(solution)/shard_map/dot_general | solution.py:71
  115.5 10.9 %all-to-all-done.1 = bf16[16,2,8192]{2,1,0:T(2,128)(2,1)S(1)} async-done(((bf16[16,2,8192]{2,1,0:T(2,128)(2,1)}), bf16[16,2,8192]{2,1,0:T(2,128)(2,1)S(1)}, u32[]{:S(2)}, u32[]{:S(2)}) %all-to-all-start.1) | async-done | bytes 524320 | tf_op jit(solution)/shard_map/all_to_all | solution.py:109
  126.4 1.8 %reshape.192 = bf16[256,1,1024]{2,1,0:T(2,128)(2,1)} reshape(bf16[16,2,8192]{2,1,0:T(2,128)(2,1)S(1)} %all-to-all-done.1) | data formatting | bytes 1048576
  128.2 1.4 %copy.50 = bf16[1,256,1024]{2,1,0:T(8,128)(2,1)S(1)} copy(bf16[1,256,1024]{2,0,1:T(2,128)(2,1)} %bitcast.63) | data formatting | bytes 1048576
  130.8 1.4 %add_convert_fusion = bf16[16,1024]{1,0:T(8,128)(2,1)} fusion(bf16[16,1024]{1,0:T(8,128)(2,1)} %reduce-scatter.5.cloned.1.call-done, f32[16,1024]{1,0:T(8,128)S(1)} %multiply_reduce_fusion, f32[16,2048]{1,0:T(8,128)S(1)} %copy-done.4, s32[]{:T(128)S(6)} %select_n.14), kind=kLoop, calls=%fused_computation.35 | loop fusion | flops 65536 | bytes 196612 | tf_op jit(solution)/shard_map/convert_element_type | solution.py:116
  (67 shorter events, 5.7 us)
Async XLA Ops:
  7.2 17.9 %copy-start = (bf16[512,2048]{1,0:T(8,128)(2,1)S(1)}, bf16[512,2048]{1,0:T(8,128)(2,1)}, u32[]{:S(2)}) copy-start(bf16[512,2048]{1,0:T(8,128)(2,1)} %param.29) | copy-start | bytes 6291460
  7.2 3.3 %copy-start.3 = (bf16[16,2048]{1,0:T(8,128)(2,1)S(1)}, bf16[16,2048]{1,0:T(8,128)(2,1)}, u32[]{:S(2)}) copy-start(bf16[16,2048]{1,0:T(8,128)(2,1)} %param.19) | copy-start | bytes 196612
  7.2 3.3 %copy-start.5 = (f32[2048]{0:T(1024)S(1)}, f32[2048]{0:T(1024)}, u32[]{:S(2)}) copy-start(f32[2048]{0:T(1024)} %param.21) | copy-start | bytes 24580
  7.2 39.6 %all-reduce.2.cloned.1.call-start = ((), (), s32[]{:S(2)}) async-start(), calls=%async_computation.4 | async-start | bytes 131072 | tf_op jit(solution)/shard_map/psum | solution.py:61
  10.5 4.1 %copy-start.8 = (f32[512]{0:T(512)S(1)}, f32[512]{0:T(512)}, u32[]{:S(2)}) copy-start(f32[512]{0:T(512)} %param.28) | copy-start | bytes 6148
  21.1 3.7 %copy-start.1 = (f32[16,4,128,128]{3,2,1,0:T(8,128)}, f32[16,4,128,128]{3,2,1,0:T(8,128)S(1)}, u32[]{:S(2)}) copy-start(f32[16,4,128,128]{3,2,1,0:T(8,128)S(1)} %multiply_add_fusion) | copy-start | bytes 12582916
  21.2 3.8 %copy-start.10 = (f32[128]{0:T(128)S(1)}, f32[128]{0:T(128)}, u32[]{:S(2)}) copy-start(f32[128]{0:T(128)} %param.23) | copy-start | bytes 1540
  24.8 1.3 copy-start.9
  24.8 23.5 %copy-start.7 = (f32[2048]{0:T(1024)S(1)}, f32[2048]{0:T(1024)}, u32[]{:S(2)}) copy-start(f32[2048]{0:T(1024)} %param.22) | copy-start | bytes 24580
  26.1 53.3 %all-gather.2.cloned.1.call-start = ((), (), s32[]{:S(2)}) async-start(), calls=%async_computation.5 | async-start | bytes 1572864 | tf_op jit(solution)/shard_map/all_gather | solution.py:99
  71.9 23.2 %reduce-scatter.3.cloned.1.call-start = ((), (), s32[]{:S(2)}) async-start(), calls=%async_computation.6 | async-start | bytes 1572864 | tf_op jit(solution)/shard_map/reduce_scatter | solution.py:106
  79.4 2.1 %copy-start.2 = (bf16[1,256,2048]{2,1,0:T(8,128)(2,1)S(1)}, bf16[1,256,2048]{2,1,0:T(8,128)(2,1)}, u32[]{:S(2)}) copy-start(bf16[1,256,2048]{2,1,0:T(8,128)(2,1)} %all-gather.2.cloned.1.call-done) | copy-start | bytes 3145732
  81.5 3.9 %copy-start.6 = (f32[16,6]{0,1:T(8,128)S(1)}, f32[16,6]{0,1:T(8,128)}, u32[]{:S(2)}) copy-start(f32[16,6]{0,1:T(8,128)} %param.31) | copy-start | bytes 1156
  104.1 22.3 %all-to-all-start.1 = ((bf16[16,2,8192]{2,1,0:T(2,128)(2,1)}), bf16[16,2,8192]{2,1,0:T(2,128)(2,1)S(1)}, u32[]{:S(2)}, u32[]{:S(2)}) async-start(bf16[16,2,8192]{2,1,0:T(2,128)(2,1)} %reshape.191), calls=%async_computation.2 | async-start | bytes 1048576 | tf_op jit(solution)/shard_map/all_to_all | solution.py:109
  110.9 19.8 %reduce-scatter.5.cloned.1.call-start = ((), (), s32[]{:S(2)}) async-start(), calls=%async_computation.7 | async-start | bytes 98304 | tf_op jit(solution)/shard_map/reduce_scatter | solution.py:72
  128.2 2.5 %copy-start.4 = (f32[16,2048]{1,0:T(8,128)S(1)}, f32[16,2048]{1,0:T(8,128)}, u32[]{:S(2)}) copy-start(f32[16,2048]{1,0:T(8,128)} %get-tuple-element.2) | copy-start | bytes 393220
Sparse Core Ops, SparseCore 0:
  26.2 20.4 all-reduce.1
  72.0 7.3 all-gather.1
  85.5 9.5 reduce-scatter.2
  115.6 8.8 reduce-scatter.4
where the time goes:
time: 140 us; the launch traced here: 139 us
  waiting for transfers between devices  47.6 us (34%)
  matrix products  23.4 us (17%)
  blocking collectives  22.2 us (16%)
  other arithmetic  14.9 us (11%)
  between operations  14.1 us (10%)
  local copies, waits for them, and re-layouts  9.27 us (7%)
  starting transfers between devices  7.14 us (5%)
    all_to_all x1, blocking collectives, local(): lax.all_to_all(outgoing, 'ep', split_axis=0, concat_axis=1, tiled=True)  22.2 us
    psum x1, waiting for transfers between devices, local(): mixer_out = lax.psum(partial_value.astype(jnp.bfloat16), 'tp')  19.7 us
    all_to_all x1, waiting for transfers between devices, local(): lax.all_to_all(expert_half, 'ep', split_axis=1, concat_axis=0, tiled=True)  10.9 us
    reduce_scatter x1, waiting for transfers between devices, local(): lax.psum_scatter(expert_part.astype(jnp.bfloat16), 'tp', scatter_dimensio...  9.58 us
    all_gather x1, waiting for transfers between devices, local(): arrived = lax.all_gather(arrived_half, 'tp', axis=2, tiled=True)  7.3 us
    all_to_all x1, starting transfers between devices, local(): lax.all_to_all(expert_half, 'ep', split_axis=1, concat_axis=0, tiled=True)  6.79 us
    unnamed x29, local copies, waits for them, and re-layouts  6.09 us
    unnamed x1, other arithmetic  4.5 us
  transfers between devices with their start and end apart: 5, of which 4 were waited for; matrix products, arithmetic and copies ran while one was open for 7% of the time, Pallas kernels for 0%

commit v1 on v0

v1 whole, which is shorter than its diff:
```python
import functools

import jax
import jax.numpy as jnp
from jax import lax
from jax.experimental import pallas as pl
from jax.experimental.pallas import tpu as pltpu
from jax.sharding import PartitionSpec as P

epsilon = 1e-06
routed_scale = 2.5
MESH = pl.DeviceIdType.MESH
f32 = jnp.float32
bf16 = jnp.bfloat16


def dot(a, b):
    return jnp.dot(a, b, preferred_element_type=f32)


def silu(v):
    return v * jax.nn.sigmoid(v)


def rms_scale(values, gain):
    return values * lax.rsqrt(jnp.mean(values * values, axis=-1, keepdims=True) + epsilon) * gain


def mixer_kernel(
    tok, gain, head_gain, bound, routes, scores, wf, wi, wq, wg, wm, st,
    partial, weights_out, new_st,
    wbuf, wmbuf, sbuf, nbuf, readout, gated, wsem, ssem, osem,
):
    seqs, heads, kdim, vdim = st.shape
    copies = [
        pltpu.make_async_copy(w, wbuf.at[i], wsem.at[i]) for i, w in enumerate((wf, wi, wq, wg))
    ]
    mix_copy = pltpu.make_async_copy(wm, wmbuf, wsem.at[4])
    state_copies = [
        pltpu.make_async_copy(st.at[:, h], sbuf.at[h], ssem.at[h]) for h in range(heads)
    ]
    for c in copies[:3] + state_copies + copies[3:] + [mix_copy]:
        c.start()
    normed = rms_scale(tok[...].astype(f32), gain[...]).astype(bf16)

    score = scores[...]
    top = score.shape[1]
    weight = score / jnp.sum(score, axis=-1, keepdims=True) * routed_scale
    named = routes[...]
    experts = weights_out.shape[0]
    wide = -(-experts // 128) * 128
    lane = lax.broadcasted_iota(jnp.int32, (seqs, wide), 1)
    dense = jnp.zeros((seqs, wide), f32)
    for t in range(top):
        dense += jnp.where(named[:, t : t + 1] == lane, weight[:, t : t + 1], 0.0)
    tall = weights_out.shape[2]
    dense = jnp.concatenate([dense, jnp.zeros((tall - seqs, wide), f32)], axis=0)
    weights_out[:, 0, :] = dense.T[:experts]

    copies[0].wait()
    forget_pre = dot(normed, wbuf[0])
    low = bound[...]
    forget = low + (1.0 - low) * jax.nn.sigmoid(forget_pre)
    key = (1.0 - low) * jax.nn.sigmoid(-forget_pre)
    copies[1].wait()
    value = dot(normed, wbuf[1])
    copies[2].wait()
    query = silu(dot(normed, wbuf[2]))
    outs = []
    for h in range(heads):
        cols = slice(h * kdim, (h + 1) * kdim)
        vcols = slice(h * vdim, (h + 1) * vdim)
        ft, kt, qt = forget[:, cols].T, key[:, cols].T, query[:, cols].T
        vh = value[:, vcols]
        state_copies[h].wait()
        for s in range(seqs):
            new = ft[:, s : s + 1] * sbuf[h, s] + kt[:, s : s + 1] * vh[s : s + 1]
            nbuf[h, s] = new
            readout[s : s + 1, vcols] = jnp.sum(new * qt[:, s : s + 1], axis=0, keepdims=True)
        out = pltpu.make_async_copy(nbuf.at[h], new_st.at[:, h], osem.at[h])
        out.start()
        outs.append(out)
    copies[3].wait()
    gate = silu(dot(normed, wbuf[3]))
    for h in range(heads):
        vcols = slice(h * vdim, (h + 1) * vdim)
        gated[:, vcols] = (
            rms_scale(readout[:, vcols], head_gain[...]) * gate[:, vcols]
        ).astype(bf16)
    mix_copy.wait()
    partial[...] = dot(gated[...], wmbuf[...]).astype(bf16)
    for out in outs:
        out.wait()


def moe_kernel(
    n_ep, n_z, tok, part_in, gain, wsrc, eg, eu, ed, sg, su, sd,
    out_ref,
    peer_part, rows, hidden, res, wgot, egb, eub, edb, sgb, sub, sdb,
    shared_send, shared_got, shared_mine, other, mine, cross, weighted, plane_got, line_send, line_got, scale_ref,
    wsem, bar_v_s, bar_v_r, ps_s, ps_r, a1_s, a1_r, a2_s, a2_r, fw_s, fw_r,
    sh_s, sh_r, x_s, x_r, g_s, g_r, l_s, l_r,
):
    n_p = n_ep // n_z
    me = lax.axis_index("ep")
    tp = lax.axis_index("tp")
    mate = 1 - tp
    z = me // n_p
    q = me % n_p
    seqs, width = tok.shape
    half = width // 2
    barrier = pltpu.get_barrier_semaphore()
    pl.semaphore_signal(barrier, inc=1, device_id=(me, mate), device_id_type=MESH)
    for k in range(1, n_ep):
        pl.semaphore_signal(
            barrier, inc=1, device_id=((me + k) % n_ep, tp), device_id_type=MESH
        )
    loads = []
    pairs = [(sg, sgb), (su, sub), (eg.at[0], egb), (eu.at[0], eub)]
    for i, (src, dst) in enumerate(pairs):
        loads.append(pltpu.make_async_copy(src, dst, wsem.at[i]))
    for c in range(2):
        loads.append(
            pltpu.make_async_copy(sd.at[:, pl.ds(c * half, half)], sdb.at[c], wsem.at[4 + c])
        )
        loads.append(
            pltpu.make_async_copy(ed.at[0, :, pl.ds(c * half, half)], edb.at[c], wsem.at[6 + c])
        )
    for c in loads:
        c.start()
    pl.semaphore_wait(barrier, n_ep)

    def send(src, dst, s, r, ep, core):
        c = pltpu.make_async_remote_copy(
            src_ref=src, dst_ref=dst, send_sem=s, recv_sem=r,
            device_id=(ep, core), device_id_type=MESH,
        )
        c.start()
        return c

    started = []
    psum = send(part_in, peer_part, ps_s, ps_r, me, mate)
    for k in range(1, n_ep):
        to = (me + k) % n_ep
        started.append(send(wsrc.at[to], wgot.at[me], bar_v_s.at[k], bar_v_r.at[k], to, tp))
    weight_copies = started[:]
    psum.wait()
    mixed = (part_in[...].astype(f32) + peer_part[...].astype(f32)).astype(bf16)
    residual = tok[...].astype(f32) + mixed.astype(f32)
    normed = rms_scale(residual, gain[...]).astype(bf16)
    own = pl.ds(pl.multiple_of(me * seqs, seqs), seqs)
    for c in range(2):
        cols = slice(c * half, (c + 1) * half)
        rows[c, own] = normed[:, cols]
        res[c] = residual[:, cols]

    def block(j):
        return rows.at[tp, pl.ds(pl.multiple_of(j * seqs, seqs), seqs)]

    line = [None]
    for d in range(1, n_z):
        to = (z + d) % n_z * n_p + q
        line.append(send(block(me), block(me), a1_s.at[d], a1_r.at[d], to, tp))
    plane = {}

    def to_plane(d):
        j = (z + n_z - d) % n_z * n_p + q
        for k in range(1, n_p):
            to = z * n_p + (q + k) % n_p
            plane[d, k] = send(
                block(j), block(j), a2_s.at[d * n_p + k], a2_r.at[d * n_p + k], to, tp
            )

    forwards = []

    def to_mate(d, k):
        j = (z + n_z - d) % n_z * n_p + (q + n_p - k) % n_p
        i = d * n_p + k
        forwards.append(send(block(j), block(j), fw_s.at[i], fw_r.at[i], me, mate))

    to_plane(0)

    loads[0].wait()
    loads[1].wait()
    shared_hidden = (silu(dot(normed, sgb[...])) * dot(normed, sub[...])).astype(bf16)
    loads[4].wait()
    loads[6].wait()
    shared_send[...] = dot(shared_hidden, sdb[mate]).astype(bf16)
    shared_copy = send(shared_send, shared_got, sh_s, sh_r, me, mate)
    shared_mine[...] = dot(shared_hidden, sdb[tp]).astype(bf16)

    for d in range(1, n_z):
        line[d].wait_recv()
        to_plane(d)
        to_mate(d, 0)
    for d in range(n_z):
        for k in range(1, n_p):
            plane[d, k].wait_recv()
            to_mate(d, k)

    for k in range(1, n_ep):
        weight_copies[k - 1].wait_recv()
    wgot[me] = wsrc[me]
    tall = wgot.shape[2]
    spread = jnp.broadcast_to(wgot[...], (n_ep, seqs, tall))
    at_lane = lax.broadcasted_iota(jnp.int32, (n_ep, seqs, tall), 2)
    at_row = lax.broadcasted_iota(jnp.int32, (n_ep, seqs, tall), 1)
    column = jnp.sum(jnp.where(at_lane == at_row, spread, 0.0), axis=2, keepdims=True)
    column = column.reshape(n_ep * seqs, 1)
    loads[2].wait()
    loads[3].wait()
    loads[5].wait()
    loads[7].wait()
    for f in forwards:
        f.wait_recv()
    left, right = rows[0], rows[1]
    gate = dot(left, egb[:half]) + dot(right, egb[half:])
    up = dot(left, eub[:half]) + dot(right, eub[half:])
    hidden[...] = (silu(gate) * up).astype(bf16)
    scale = jnp.broadcast_to(column, (n_ep * seqs, 128))

    chunk = n_p * seqs
    order = list(range(1, n_z)) + [0]
    crossing = {}
    scale_ref[...] = scale
    for d in order:
        at = pl.ds(pl.multiple_of((z + d) % n_z * chunk, chunk), chunk)
        h = hidden[at]
        other[d] = dot(h, edb[mate]).astype(bf16)
        crossing[d] = send(other.at[d], cross.at[d], x_s.at[d], x_r.at[d], me, mate)
        mine[d] = dot(h, edb[tp]).astype(bf16)
    returns = {}
    for d in order:
        at = pl.ds(pl.multiple_of((z + d) % n_z * chunk, chunk), chunk)
        crossing[d].wait_recv()
        whole = (mine[d].astype(f32) + cross[d].astype(f32)).astype(bf16).astype(f32)
        weighted[d] = (whole * scale_ref[at, 0:1]).astype(bf16)
        for k in range(1, n_p):
            to = (q + k) % n_p
            src = weighted.at[d, pl.ds(pl.multiple_of(to * seqs, seqs), seqs)]
            i = d * n_p + k
            returns[d, k] = send(src, plane_got.at[i], g_s.at[i], g_r.at[i], z * n_p + to, tp)
    mine_at = pl.ds(pl.multiple_of(q * seqs, seqs), seqs)
    lines = {}
    total = None
    for d in order:
        total = weighted[d, mine_at].astype(f32)
        for k in range(1, n_p):
            returns[d, k].wait_recv()
            total += plane_got[d * n_p + k].astype(f32)
        if d > 0:
            sums = line_send.at[d]
            line_send[d] = total.astype(bf16)
            lines[d] = send(
                sums, line_got.at[d], l_s.at[d], l_r.at[d], (z + d) % n_z * n_p + q, tp
            )
    shared_copy.wait_recv()
    shared = (shared_mine[...].astype(f32) + shared_got[...].astype(f32)).astype(bf16)
    for d in range(1, n_z):
        lines[d].wait_recv()
        total += line_got[d].astype(f32)
    out_ref[...] = (res[tp] + total + shared.astype(f32)).astype(bf16)
    everything = started + line[1:] + list(plane.values()) + forwards
    everything += list(crossing.values()) + list(returns.values()) + list(lines.values())
    for c in everything + [shared_copy]:
        c.wait_send()


def local(n_ep, *args):
    (
        tokens, state, mix_gain, moe_gain, head_gain, w_forget, w_query, w_input, w_outgate,
        lower_bound, w_mix_out, routes, route_scores, expert_gate, expert_up, expert_down,
        shared_gate, shared_up, shared_down,
    ) = args
    seqs, width = tokens.shape
    heads, kdim, vdim = state.shape[1:]
    half = width // 2
    n_z = max(d for d in range(1, n_ep + 1) if d * d <= n_ep and n_ep % d == 0)
    n_p = n_ep // n_z
    experts = expert_gate.shape[0] * n_ep
    tall = -(-seqs // 128) * 128
    vmem = pl.BlockSpec(memory_space=pltpu.VMEM)
    anym = pl.BlockSpec(memory_space=pl.ANY)
    dma = pltpu.SemaphoreType.DMA
    inner = heads * vdim
    partial, dense, new_state = pl.pallas_call(
        mixer_kernel,
        out_shape=(
            jax.ShapeDtypeStruct((seqs, width), bf16),
            jax.ShapeDtypeStruct((experts, 1, tall), f32),
            jax.ShapeDtypeStruct(state.shape, f32),
        ),
        in_specs=[vmem] * 6 + [anym] * 6,
        out_specs=(vmem, vmem, anym),
        scratch_shapes=[
            pltpu.VMEM((4,) + w_forget.shape, bf16),
            pltpu.VMEM(w_mix_out.shape, bf16),
            pltpu.VMEM((heads, seqs, kdim, vdim), f32),
            pltpu.VMEM((heads, seqs, kdim, vdim), f32),
            pltpu.VMEM((seqs, inner), f32),
            pltpu.VMEM((seqs, inner), bf16),
            dma((5,)),
            dma((heads,)),
            dma((heads,)),
        ],
        name="mixer",
    )(
        tokens, mix_gain.reshape(1, -1), head_gain.reshape(1, -1), lower_bound.reshape(1, -1),
        routes, route_scores, w_forget, w_input, w_query, w_outgate, w_mix_out, state,
    )
    hid = expert_gate.shape[2]
    shid = shared_gate.shape[1]
    chunk = n_p * seqs
    layer_out = pl.pallas_call(
        functools.partial(moe_kernel, n_ep, n_z),
        out_shape=jax.ShapeDtypeStruct((seqs, half), bf16),
        in_specs=[vmem] * 4 + [anym] * 6,
        out_specs=vmem,
        scratch_shapes=[
            pltpu.VMEM((seqs, width), bf16),
            pltpu.VMEM((2, n_ep * seqs, half), bf16),
            pltpu.VMEM((n_ep * seqs, hid), bf16),
            pltpu.VMEM((2, seqs, half), f32),
            pltpu.VMEM((n_ep, 1, tall), f32),
            pltpu.VMEM((width, hid), bf16),
            pltpu.VMEM((width, hid), bf16),
            pltpu.VMEM((2, hid, half), bf16),
            pltpu.VMEM((width, shid), bf16),
            pltpu.VMEM((width, shid), bf16),
            pltpu.VMEM((2, shid, half), bf16),
            pltpu.VMEM((seqs, half), bf16),
            pltpu.VMEM((seqs, half), bf16),
            pltpu.VMEM((seqs, half), bf16),
            pltpu.VMEM((n_z, chunk, half), bf16),
            pltpu.VMEM((n_z, chunk, half), bf16),
            pltpu.VMEM((n_z, chunk, half), bf16),
            pltpu.VMEM((n_z, chunk, half), bf16),
            pltpu.VMEM((n_ep, seqs, half), bf16),
            pltpu.VMEM((n_z, seqs, half), bf16),
            pltpu.VMEM((n_z, seqs, half), bf16),
            pltpu.VMEM((n_ep * seqs, 128), f32),
            dma((8,)),
            dma((n_ep,)), dma((n_ep,)),
            dma, dma,
            dma((n_z,)), dma((n_z,)),
            dma((n_ep,)), dma((n_ep,)),
            dma((n_ep,)), dma((n_ep,)),
            dma, dma,
            dma((n_z,)), dma((n_z,)),
            dma((n_ep,)), dma((n_ep,)),
            dma((n_z,)), dma((n_z,)),
        ],
        compiler_params=pltpu.CompilerParams(collective_id=0, has_side_effects=True),
        name="experts",
    )(
        tokens, partial, moe_gain.reshape(1, -1), dense,
        expert_gate, expert_up, expert_down, shared_gate, shared_up, shared_down,
    )
    return (layer_out, new_state)


def solution(mesh):
    return jax.shard_map(
        functools.partial(local, mesh.shape["ep"]),
        mesh=mesh,
        in_specs=(
            P("ep", None),
            P("ep", "tp", None, None),
            P(),
            P(),
            P(),
            P(None, "tp"),
            P(None, "tp"),
            P(None, "tp"),
            P(None, "tp"),
            P("tp"),
            P("tp", None),
            P("ep", None),
            P("ep", None),
            P("ep", None, "tp"),
            P("ep", None, "tp"),
            P("ep", "tp", None),
            P(None, "tp"),
            P(None, "tp"),
            P("tp", None),
        ),
        out_specs=(P("ep", "tp"), P("ep", "tp", None, None)),
        check_vma=False,
    )
```

time: 140 us -> 47.9 us (0.34)
  waiting for transfers between devices: 47.6 us -> 0 us
  Pallas kernels: 0 us -> 42.8 us
  matrix products: 23.4 us -> 0 us
  blocking collectives: 22.2 us -> 0 us
  other arithmetic: 14.9 us -> 0 us
  between operations: 14.1 us -> 0.65 us
  starting transfers between devices: 7.14 us -> 0 us
  local copies, waits for them, and re-layouts: 9.27 us -> 4.1 us
    pallas_call x0 -> x2, Pallas kernels: none -> 42.8 us  [the longest x1 32.8 us: local(): pl.pallas_call(functools.partial(moe_kernel, n_ep, n_z), out_shape=jax.Sh...]
    dot_general x11 -> x0, matrix products: 23.4 us -> none  [the longest x1 3.82 us: local(): jnp.einsum('esf,efd->esd', expert_hidden, expert_down, preferred_element_...]
    all_to_all x1 -> x0, blocking collectives: 22.2 us -> none  [local(): lax.all_to_all(outgoing, 'ep', split_axis=0, concat_axis=1, tiled=True)]
    psum x1 -> x0, waiting for transfers between devices: 19.7 us -> none  [local(): mixer_out = lax.psum(partial_value.astype(jnp.bfloat16), 'tp')]
    all_to_all x1 -> x0, waiting for transfers between devices: 10.9 us -> none  [local(): lax.all_to_all(expert_half, 'ep', split_axis=1, concat_axis=0, tiled=True)]
    reduce_scatter x2 -> x0, waiting for transfers between devices: 9.6 us -> none  [the longest x1 9.58 us: local(): lax.psum_scatter(expert_part.astype(jnp.bfloat16), 'tp', scatter_dimensio...]
    all_gather x1 -> x0, waiting for transfers between devices: 7.3 us -> none  [local(): arrived = lax.all_gather(arrived_half, 'tp', axis=2, tiled=True)]
    all_to_all x1 -> x0, starting transfers between devices: 6.79 us -> none  [local(): lax.all_to_all(expert_half, 'ep', split_axis=1, concat_axis=0, tiled=True)]
  transfers between devices with their start and end apart: 5 -> 0, of which waited for: 4 -> 0; matrix products, arithmetic and copies ran while one was open for 7% -> 0% of each run, Pallas kernels for 0% -> 0%
where the time goes in v1:
time: 47.9 us; the launch traced here: 47.6 us
  Pallas kernels  42.8 us (89%)
  local copies, waits for them, and re-layouts  4.1 us (9%)
  between operations  0.65 us (1%)
    pallas_call x1, Pallas kernels, local(): pl.pallas_call(functools.partial(moe_kernel, n_ep, n_z), out_shape=jax.Sh...  32.8 us
    pallas_call x1, Pallas kernels, local(): pl.pallas_call(mixer_kernel, out_shape=(jax.ShapeDtypeStruct((seqs, width...  10.1 us
    unnamed x3, local copies, waits for them, and re-layouts  4.1 us

profile of v1, /device:TPU:0, one launch (start us, length us, event | category | flops | bytes accessed | tf_op | source)
XLA Modules:
  0.0 47.6 jit_solution(3896301001229793084)
XLA Ops:
  0.6 1.4 %copy.21.routes = s32[16,6]{1,0:T(8,128)} copy(s32[16,6]{0,1:T(8,128)} %param.30) | data formatting | bytes 768 | tf_op args[11]
  2.0 1.4 %copy.22.scores = f32[16,6]{1,0:T(8,128)} copy(f32[16,6]{0,1:T(8,128)} %param.31) | data formatting | bytes 768 | tf_op args[12]
  3.4 10.1 %mixer.1 = (bf16[16,2048]{1,0:T(8,128)(2,1)}, f32[16,1,128]{2,1,0:T(1,128)}, f32[16,4,128,128]{3,2,1,0:T(8,128)}) custom-call(bf16[16,2048]{1,0:T(8,128)(2,1)} %tok.3, f32[1,2048]{1,0:T(1,128)} %bitcast.4, f32[1,128]{1,0:T(1,128)} %bitcast.7, f32[1,512]{1,0:T(1,128)} %bitcast.6, s32[16,6]{1,0:T(8,128)} %copy.21.routes, f32[16,6]{1,0:T(8,128)} %copy.22.scores, ...), custom_call_target="tpu_custom_call" | custom-call | tf_op jit(solution)/shard_map/mixer/pallas_call | solution.py:286
  13.4 32.8 %experts.1 = bf16[16,1024]{1,0:T(8,128)(2,1)} custom-call(bf16[16,2048]{1,0:T(8,128)(2,1)} %tok.3, bf16[16,2048]{1,0:T(8,128)(2,1)} %get-tuple-element.5.part_in, f32[1,2048]{1,0:T(1,128)} %bitcast.5, f32[16,1,128]{2,1,0:T(1,128)} %get-tuple-element.6.wsrc, bf16[1,2048,256]{2,1,0:T(8,128)(2,1)} %eg.1, bf16[1,2048,256]{2,1,0:T(8,128)(2,1)} %eu.1, ...), custom_call_target="tpu_custom_call" | custom-call | tf_op jit(solution)/shard_map/experts/pallas_call | solution.py:314
  46.2 1.4 %copy.24 = bf16[16,1024]{1,0:T(8,128)(2,1)} copy(bf16[16,1024]{1,0:T(8,128)(2,1)} %experts.1) | data formatting | bytes 65536

commit v2 on v1

--- a/solution.py
+++ b/solution.py
@@ -27,35 +27,33 @@
 
 
 def mixer_kernel(
-    tok, gain, head_gain, bound, routes, scores, wf, wi, wq, wg, wm, st,
-    partial, weights_out, new_st,
-    wbuf, wmbuf, sbuf, nbuf, readout, gated, wsem, ssem, osem,
+    tok, gain, bound, routes, scores, wf, wi, wq, st,
+    normed_out, readout, weights_out, new_st,
+    wbuf, sbuf, nbuf, wsem, ssem, osem,
 ):
     seqs, heads, kdim, vdim = st.shape
     copies = [
-        pltpu.make_async_copy(w, wbuf.at[i], wsem.at[i]) for i, w in enumerate((wf, wi, wq, wg))
+        pltpu.make_async_copy(w, wbuf.at[i], wsem.at[i]) for i, w in enumerate((wf, wi, wq))
     ]
-    mix_copy = pltpu.make_async_copy(wm, wmbuf, wsem.at[4])
     state_copies = [
         pltpu.make_async_copy(st.at[:, h], sbuf.at[h], ssem.at[h]) for h in range(heads)
     ]
-    for c in copies[:3] + state_copies + copies[3:] + [mix_copy]:
+    for c in copies + state_copies:
         c.start()
     normed = rms_scale(tok[...].astype(f32), gain[...]).astype(bf16)
+    normed_out[...] = normed
 
     score = scores[...]
-    top = score.shape[1]
-    weight = score / jnp.sum(score, axis=-1, keepdims=True) * routed_scale
+    top = score.shape[0]
+    weight = score / jnp.sum(score, axis=0, keepdims=True) * routed_scale
     named = routes[...]
     experts = weights_out.shape[0]
-    wide = -(-experts // 128) * 128
-    lane = lax.broadcasted_iota(jnp.int32, (seqs, wide), 1)
-    dense = jnp.zeros((seqs, wide), f32)
+    number = lax.broadcasted_iota(jnp.int32, (experts, seqs), 0)
+    dense = jnp.zeros((experts, seqs), f32)
     for t in range(top):
-        dense += jnp.where(named[:, t : t + 1] == lane, weight[:, t : t + 1], 0.0)
+        dense += jnp.where(named[t : t + 1] == number, weight[t : t + 1], 0.0)
     tall = weights_out.shape[2]
-    dense = jnp.concatenate([dense, jnp.zeros((tall - seqs, wide), f32)], axis=0)
-    weights_out[:, 0, :] = dense.T[:experts]
+    weights_out[:, 0, :] = jnp.concatenate([dense, jnp.zeros((experts, tall - seqs), f32)], axis=1)
 
     copies[0].wait()
     forget_pre = dot(normed, wbuf[0])
@@ -80,23 +78,14 @@
         out = pltpu.make_async_copy(nbuf.at[h], new_st.at[:, h], osem.at[h])
         out.start()
         outs.append(out)
-    copies[3].wait()
-    gate = silu(dot(normed, wbuf[3]))
-    for h in range(heads):
-        vcols = slice(h * vdim, (h + 1) * vdim)
-        gated[:, vcols] = (
-            rms_scale(readout[:, vcols], head_gain[...]) * gate[:, vcols]
-        ).astype(bf16)
-    mix_copy.wait()
-    partial[...] = dot(gated[...], wmbuf[...]).astype(bf16)
     for out in outs:
         out.wait()
 
 
 def moe_kernel(
-    n_ep, n_z, tok, part_in, gain, wsrc, eg, eu, ed, sg, su, sd,
+    n_ep, n_z, tok, mixer_in, readout, head_gain, gain, wsrc, wg, wm, eg, eu, ed, sg, su, sd,
     out_ref,
-    peer_part, rows, hidden, res, wgot, egb, eub, edb, sgb, sub, sdb,
+    wgb, wmb, gated, part_in, peer_part, rows, res, wgot, egb, eub, edb, sgb, sub, sdb,
     shared_send, shared_got, shared_mine, other, mine, cross, weighted, plane_got, line_send, line_got, scale_ref,
     wsem, bar_v_s, bar_v_r, ps_s, ps_r, a1_s, a1_r, a2_s, a2_r, fw_s, fw_r,
     sh_s, sh_r, x_s, x_r, g_s, g_r, l_s, l_r,
@@ -115,6 +104,10 @@
         pl.semaphore_signal(
             barrier, inc=1, device_id=((me + k) % n_ep, tp), device_id_type=MESH
         )
+    gate_load = pltpu.make_async_copy(wg, wgb, wsem.at[8])
+    mix_load = pltpu.make_async_copy(wm, wmb, wsem.at[9])
+    gate_load.start()
+    mix_load.start()
     loads = []
     pairs = [(sg, sgb), (su, sub), (eg.at[0], egb), (eu.at[0], eub)]
     for i, (src, dst) in enumerate(pairs):
@@ -128,6 +121,16 @@
         )
     for c in loads:
         c.start()
+    gate_load.wait()
+    open_gate = silu(dot(mixer_in[...], wgb[...]))
+    vdim = head_gain.shape[1]
+    for h in range(readout.shape[1] // vdim):
+        vcols = slice(h * vdim, (h + 1) * vdim)
+        gated[:, vcols] = (
+            rms_scale(readout[:, vcols], head_gain[...]) * open_gate[:, vcols]
+        ).astype(bf16)
+    mix_load.wait()
+    part_in[...] = dot(gated[...], wmb[...]).astype(bf16)
     pl.semaphore_wait(barrier, n_ep)
 
     def send(src, dst, s, r, ep, core):
@@ -171,12 +174,12 @@
                 block(j), block(j), a2_s.at[d * n_p + k], a2_r.at[d * n_p + k], to, tp
             )
 
-    forwards = []
+    forwards = {}
 
     def to_mate(d, k):
         j = (z + n_z - d) % n_z * n_p + (q + n_p - k) % n_p
         i = d * n_p + k
-        forwards.append(send(block(j), block(j), fw_s.at[i], fw_r.at[i], me, mate))
+        forwards[d, k] = send(block(j), block(j), fw_s.at[i], fw_r.at[i], me, mate)
 
     to_plane(0)
 
@@ -193,11 +196,6 @@
         line[d].wait_recv()
         to_plane(d)
         to_mate(d, 0)
-    for d in range(n_z):
-        for k in range(1, n_p):
-            plane[d, k].wait_recv()
-            to_mate(d, k)
-
     for k in range(1, n_ep):
         weight_copies[k - 1].wait_recv()
     wgot[me] = wsrc[me]
@@ -211,39 +209,48 @@
     loads[3].wait()
     loads[5].wait()
     loads[7].wait()
-    for f in forwards:
-        f.wait_recv()
-    left, right = rows[0], rows[1]
-    gate = dot(left, egb[:half]) + dot(right, egb[half:])
-    up = dot(left, eub[:half]) + dot(right, eub[half:])
-    hidden[...] = (silu(gate) * up).astype(bf16)
-    scale = jnp.broadcast_to(column, (n_ep * seqs, 128))
-
+    scale_ref[...] = jnp.broadcast_to(column, (n_ep * seqs, 128))
     chunk = n_p * seqs
-    order = list(range(1, n_z)) + [0]
     crossing = {}
-    scale_ref[...] = scale
-    for d in order:
-        at = pl.ds(pl.multiple_of((z + d) % n_z * chunk, chunk), chunk)
-        h = hidden[at]
-        other[d] = dot(h, edb[mate]).astype(bf16)
-        crossing[d] = send(other.at[d], cross.at[d], x_s.at[d], x_r.at[d], me, mate)
-        mine[d] = dot(h, edb[tp]).astype(bf16)
     returns = {}
-    for d in order:
-        at = pl.ds(pl.multiple_of((z + d) % n_z * chunk, chunk), chunk)
-        crossing[d].wait_recv()
-        whole = (mine[d].astype(f32) + cross[d].astype(f32)).astype(bf16).astype(f32)
-        weighted[d] = (whole * scale_ref[at, 0:1]).astype(bf16)
+
+    def rows_of(r):
+        return pl.ds(pl.multiple_of((z + r) % n_z * chunk, chunk), chunk)
+
+    def give_back(r):
+        crossing[r].wait_recv()
+        whole = (mine[r].astype(f32) + cross[r].astype(f32)).astype(bf16).astype(f32)
+        weighted[r] = (whole * scale_ref[rows_of(r), 0:1]).astype(bf16)
         for k in range(1, n_p):
             to = (q + k) % n_p
-            src = weighted.at[d, pl.ds(pl.multiple_of(to * seqs, seqs), seqs)]
-            i = d * n_p + k
-            returns[d, k] = send(src, plane_got.at[i], g_s.at[i], g_r.at[i], z * n_p + to, tp)
+            src = weighted.at[r, pl.ds(pl.multiple_of(to * seqs, seqs), seqs)]
+            i = r * n_p + k
+            returns[r, k] = send(src, plane_got.at[i], g_s.at[i], g_r.at[i], z * n_p + to, tp)
+
+    arrival = [(n_z - d) % n_z for d in range(n_z)]
+    for d in range(n_z):
+        r = arrival[d]
+        for k in range(1, n_p):
+            plane[d, k].wait_recv()
+            to_mate(d, k)
+        for k in range(n_p):
+            if d > 0 or k > 0:
+                forwards[d, k].wait_recv()
+        at = rows_of(r)
+        left, right = rows[0, at], rows[1, at]
+        gate = dot(left, egb[:half]) + dot(right, egb[half:])
+        up = dot(left, eub[:half]) + dot(right, eub[half:])
+        h = (silu(gate) * up).astype(bf16)
+        other[r] = dot(h, edb[mate]).astype(bf16)
+        crossing[r] = send(other.at[r], cross.at[r], x_s.at[r], x_r.at[r], me, mate)
+        mine[r] = dot(h, edb[tp]).astype(bf16)
+        if d > 0:
+            give_back(arrival[d - 1])
+    give_back(arrival[n_z - 1])
     mine_at = pl.ds(pl.multiple_of(q * seqs, seqs), seqs)
     lines = {}
     total = None
-    for d in order:
+    for d in arrival[1:] + [0]:
         total = weighted[d, mine_at].astype(f32)
         for k in range(1, n_p):
             returns[d, k].wait_recv()
@@ -260,7 +267,7 @@
         lines[d].wait_recv()
         total += line_got[d].astype(f32)
     out_ref[...] = (res[tp] + total + shared.astype(f32)).astype(bf16)
-    everything = started + line[1:] + list(plane.values()) + forwards
+    everything = started + line[1:] + list(plane.values()) + list(forwards.values())
     everything += list(crossing.values()) + list(returns.values()) + list(lines.values())
     for c in everything + [shared_copy]:
         c.wait_send()
@@ -283,30 +290,28 @@
     anym = pl.BlockSpec(memory_space=pl.ANY)
     dma = pltpu.SemaphoreType.DMA
     inner = heads * vdim
-    partial, dense, new_state = pl.pallas_call(
+    normed, readout, dense, new_state = pl.pallas_call(
         mixer_kernel,
         out_shape=(
             jax.ShapeDtypeStruct((seqs, width), bf16),
+            jax.ShapeDtypeStruct((seqs, inner), f32),
             jax.ShapeDtypeStruct((experts, 1, tall), f32),
             jax.ShapeDtypeStruct(state.shape, f32),
         ),
-        in_specs=[vmem] * 6 + [anym] * 6,
-        out_specs=(vmem, vmem, anym),
+        in_specs=[vmem] * 5 + [anym] * 4,
+        out_specs=(vmem, vmem, vmem, anym),
         scratch_shapes=[
-            pltpu.VMEM((4,) + w_forget.shape, bf16),
-            pltpu.VMEM(w_mix_out.shape, bf16),
+            pltpu.VMEM((3,) + w_forget.shape, bf16),
             pltpu.VMEM((heads, seqs, kdim, vdim), f32),
             pltpu.VMEM((heads, seqs, kdim, vdim), f32),
-            pltpu.VMEM((seqs, inner), f32),
-            pltpu.VMEM((seqs, inner), bf16),
-            dma((5,)),
+            dma((3,)),
             dma((heads,)),
             dma((heads,)),
         ],
         name="mixer",
     )(
-        tokens, mix_gain.reshape(1, -1), head_gain.reshape(1, -1), lower_bound.reshape(1, -1),
-        routes, route_scores, w_forget, w_input, w_query, w_outgate, w_mix_out, state,
+        tokens, mix_gain.reshape(1, -1), lower_bound.reshape(1, -1), routes.T, route_scores.T,
+        w_forget, w_input, w_query, state,
     )
     hid = expert_gate.shape[2]
     shid = shared_gate.shape[1]
@@ -314,12 +319,15 @@
     layer_out = pl.pallas_call(
         functools.partial(moe_kernel, n_ep, n_z),
         out_shape=jax.ShapeDtypeStruct((seqs, half), bf16),
-        in_specs=[vmem] * 4 + [anym] * 6,
+        in_specs=[vmem] * 6 + [anym] * 8,
         out_specs=vmem,
         scratch_shapes=[
+            pltpu.VMEM(w_outgate.shape, bf16),
+            pltpu.VMEM(w_mix_out.shape, bf16),
+            pltpu.VMEM((seqs, inner), bf16),
+            pltpu.VMEM((seqs, width), bf16),
             pltpu.VMEM((seqs, width), bf16),
             pltpu.VMEM((2, n_ep * seqs, half), bf16),
-            pltpu.VMEM((n_ep * seqs, hid), bf16),
             pltpu.VMEM((2, seqs, half), f32),
             pltpu.VMEM((n_ep, 1, tall), f32),
             pltpu.VMEM((width, hid), bf16),
@@ -339,7 +347,7 @@
             pltpu.VMEM((n_z, seqs, half), bf16),
             pltpu.VMEM((n_z, seqs, half), bf16),
             pltpu.VMEM((n_ep * seqs, 128), f32),
-            dma((8,)),
+            dma((10,)),
             dma((n_ep,)), dma((n_ep,)),
             dma, dma,
             dma((n_z,)), dma((n_z,)),
@@ -353,8 +361,8 @@
         compiler_params=pltpu.CompilerParams(collective_id=0, has_side_effects=True),
         name="experts",
     )(
-        tokens, partial, moe_gain.reshape(1, -1), dense,
-        expert_gate, expert_up, expert_down, shared_gate, shared_up, shared_down,
+        tokens, normed, readout, head_gain.reshape(1, -1), moe_gain.reshape(1, -1), dense,
+        w_outgate, w_mix_out, expert_gate, expert_up, expert_down, shared_gate, shared_up, shared_down,
     )
     return (layer_out, new_state)
 

time: 47.9 us -> 45.4 us (0.948)
  local copies, waits for them, and re-layouts: 4.1 us -> 1.38 us
    unnamed x3 -> x1, local copies, waits for them, and re-layouts: 4.1 us -> 1.38 us
    pallas_call x1, Pallas kernels: 10.1 us -> 10.6 us  [local(): pl.pallas_call(mixer_kernel, out_shape=(jax.ShapeDtypeStruct((seqs, width...]
where the time goes in v2:
time: 45.4 us; the launch traced here: 45.1 us
  Pallas kernels  43.1 us (95%)
  local copies, waits for them, and re-layouts  1.38 us (3%)
  between operations  0.65 us (1%)
    pallas_call x1, Pallas kernels, local(): pl.pallas_call(functools.partial(moe_kernel, n_ep, n_z), out_shape=jax.Sh...  32.4 us
    pallas_call x1, Pallas kernels, local(): pl.pallas_call(mixer_kernel, out_shape=(jax.ShapeDtypeStruct((seqs, width...  10.6 us
    unnamed x1, local copies, waits for them, and re-layouts  1.38 us

profile of v2, /device:TPU:0, one launch (start us, length us, event | category | flops | bytes accessed | tf_op | source)
XLA Modules:
  0.0 45.1 jit_solution(13812340653442519559)
XLA Ops:
  0.6 10.6 %mixer.1 = (bf16[16,2048]{1,0:T(8,128)(2,1)}, f32[16,512]{1,0:T(8,128)}, f32[16,1,128]{2,1,0:T(1,128)}, f32[16,4,128,128]{3,2,1,0:T(8,128)}) custom-call(bf16[16,2048]{1,0:T(8,128)(2,1)} %tok.3, f32[1,2048]{1,0:T(1,128)} %bitcast.6, f32[1,512]{1,0:T(1,128)} %bitcast.10, s32[6,16]{1,0:T(8,128)} %bitcast.8, f32[6,16]{1,0:T(8,128)} %bitcast.9, ...), custom_call_target="tpu_custom_call" | custom-call | tf_op jit(solution)/shard_map/mixer/pallas_call | solution.py:293
  11.3 32.4 %experts.1 = bf16[16,1024]{1,0:T(8,128)(2,1)} custom-call(bf16[16,2048]{1,0:T(8,128)(2,1)} %tok.3, bf16[16,2048]{1,0:T(8,128)(2,1)} %get-tuple-element.6.mixer_in, f32[16,512]{1,0:T(8,128)} %get-tuple-element.7.readout, f32[1,128]{1,0:T(1,128)} %bitcast.11, f32[1,2048]{1,0:T(1,128)} %bitcast.7, f32[16,1,128]{2,1,0:T(1,128)} %get-tuple-element.8.wsrc, ...), custom_call_target="tpu_custom_call" | custom-call | tf_op jit(solution)/shard_map/experts/pallas_call | solution.py:319
  43.7 1.4 %copy.22 = bf16[16,1024]{1,0:T(8,128)(2,1)} copy(bf16[16,1024]{1,0:T(8,128)(2,1)} %experts.1) | data formatting | bytes 65536

commit v3 on v2

--- a/solution.py
+++ b/solution.py
@@ -59,7 +59,6 @@
     forget_pre = dot(normed, wbuf[0])
     low = bound[...]
     forget = low + (1.0 - low) * jax.nn.sigmoid(forget_pre)
-    key = (1.0 - low) * jax.nn.sigmoid(-forget_pre)
     copies[1].wait()
     value = dot(normed, wbuf[1])
     copies[2].wait()
@@ -68,11 +67,12 @@
     for h in range(heads):
         cols = slice(h * kdim, (h + 1) * kdim)
         vcols = slice(h * vdim, (h + 1) * vdim)
-        ft, kt, qt = forget[:, cols].T, key[:, cols].T, query[:, cols].T
+        ft, qt = forget[:, cols].T, query[:, cols].T
         vh = value[:, vcols]
         state_copies[h].wait()
         for s in range(seqs):
-            new = ft[:, s : s + 1] * sbuf[h, s] + kt[:, s : s + 1] * vh[s : s + 1]
+            row = vh[s : s + 1]
+            new = row + ft[:, s : s + 1] * (sbuf[h, s] - row)
             nbuf[h, s] = new
             readout[s : s + 1, vcols] = jnp.sum(new * qt[:, s : s + 1], axis=0, keepdims=True)
         out = pltpu.make_async_copy(nbuf.at[h], new_st.at[:, h], osem.at[h])

time: 45.4 us -> 44.3 us (0.976)
  Pallas kernels: 43.1 us -> 42 us
    pallas_call x1, Pallas kernels: 10.6 us -> 9.54 us  [local(): pl.pallas_call(mixer_kernel, out_shape=(jax.ShapeDtypeStruct((seqs, width...]
where the time goes in v3:
time: 44.3 us; the launch traced here: 44 us
  Pallas kernels  42 us (95%)
  local copies, waits for them, and re-layouts  1.38 us (3%)
  between operations  0.65 us (1%)
    pallas_call x1, Pallas kernels, local(): pl.pallas_call(functools.partial(moe_kernel, n_ep, n_z), out_shape=jax.Sh...  32.4 us
    pallas_call x1, Pallas kernels, local(): pl.pallas_call(mixer_kernel, out_shape=(jax.ShapeDtypeStruct((seqs, width...  9.54 us
    unnamed x1, local copies, waits for them, and re-layouts  1.38 us

profile of v3, /device:TPU:0, one launch (start us, length us, event | category | flops | bytes accessed | tf_op | source)
XLA Modules:
  0.0 44.0 jit_solution(14735730251785427152)
XLA Ops:
  0.6 9.5 %mixer.1 = (bf16[16,2048]{1,0:T(8,128)(2,1)}, f32[16,512]{1,0:T(8,128)}, f32[16,1,128]{2,1,0:T(1,128)}, f32[16,4,128,128]{3,2,1,0:T(8,128)}) custom-call(bf16[16,2048]{1,0:T(8,128)(2,1)} %tok.3, f32[1,2048]{1,0:T(1,128)} %bitcast.6, f32[1,512]{1,0:T(1,128)} %bitcast.10, s32[6,16]{1,0:T(8,128)} %bitcast.8, f32[6,16]{1,0:T(8,128)} %bitcast.9, ...), custom_call_target="tpu_custom_call" | custom-call | tf_op jit(solution)/shard_map/mixer/pallas_call | solution.py:293
  10.2 32.4 %experts.1 = bf16[16,1024]{1,0:T(8,128)(2,1)} custom-call(bf16[16,2048]{1,0:T(8,128)(2,1)} %tok.3, bf16[16,2048]{1,0:T(8,128)(2,1)} %get-tuple-element.6.mixer_in, f32[16,512]{1,0:T(8,128)} %get-tuple-element.7.readout, f32[1,128]{1,0:T(1,128)} %bitcast.11, f32[1,2048]{1,0:T(1,128)} %bitcast.7, f32[16,1,128]{2,1,0:T(1,128)} %get-tuple-element.8.wsrc, ...), custom_call_target="tpu_custom_call" | custom-call | tf_op jit(solution)/shard_map/experts/pallas_call | solution.py:319
  42.6 1.4 %copy.22 = bf16[16,1024]{1,0:T(8,128)(2,1)} copy(bf16[16,1024]{1,0:T(8,128)(2,1)} %experts.1) | data formatting | bytes 65536
